TPU v7x, 32 devices: a whole 2x2x4 slice. The times are simulated.
32 devices in a mesh: sp: 4 (over y, x), tp: 8 (over z, core).
Axes of the slice: x: 2, y: 2, z: 4, core: 2. Of those that a mesh axis runs over, the one named last changes fastest.
Arguments:
- queries: bfloat16 [2048, 2048], P('sp', 'tp'), may hold values from -8 to 8
- keys: bfloat16 [2048, 1024], P('sp', 'tp'), may hold values from -8 to 8
- values: bfloat16 [2048, 1024], P('sp', 'tp'), may hold values from -6 to 6
- doc_ids: int32 [2048], P('sp'), may hold values from 0 to 1, never falling along the last dimension, each value on 1 to 1536 neighbouring positions
- sink_logits: float32 [32], P('tp'), may hold values from 3 to 6
- out_weight: bfloat16 [2048, 2048], P('tp'), may hold values from -0.75 to 0.75
- residual: bfloat16 [2048, 2048], P(('sp', 'tp')), may hold values from -6 to 6
- norm_gain: float32 [2048], replicated, may hold values from 0.1 to 1.9
- routes: int32 [2048, 2], P(('sp', 'tp')), may hold values from 0 to 3, all different within a row; in each aligned block of 64 rows (0 to 63, 64 to 127, ...) at most 36 rows name the same one
- route_weights: float32 [2048, 2], P(('sp', 'tp')), may hold values from 0.2 to 1
- gate_weight: bfloat16 [4, 2048, 7168], P('sp', None, 'tp'), may hold values from -0.125 to 0.125
- up_weight: bfloat16 [4, 2048, 7168], P('sp', None, 'tp'), may hold values from -0.125 to 0.125
- down_weight: bfloat16 [4, 7168, 2048], P('sp', 'tp'), may hold values from -0.0625 to 0.0625
Outputs:
- layer_output: bfloat16 [2048, 2048], P(('sp', 'tp'))
Inputs may be any that keep to these rules, and one draw needn't show every extreme that they name: `doc_ids`: never falling along the sequence; each document spans 1 to 1536 positions, one exactly that many. `routes`: each row names 2 different experts. In the rows of one device (aligned blocks of 64 rows) no expert is named by more than 36 rows, a bound that some block reaches.
All inputs are finite; a program needn't handle non-finite values.
Results may differ from a plain program's by a relative error of at most 0.015.
Values may be sent and summed in bfloat16 or wider, within the bound.
No kernel may reach another device: no remote copies, remote signals or barrier semaphores. Data moves between devices by JAX's collectives and lax.ppermute only.
A program may use at most 128 MiB of HBM per device.

v0:
```python
import math

import jax
import jax.numpy as jnp
from jax import lax
from jax.sharding import PartitionSpec as P

HEAD_DIM = 64
WINDOW = 128


layer_epsilon = 1e-05
masked_score = -1e30


def passed_along(value, axis, steps):
    count = lax.axis_size(axis)
    first, last = (max(0, -steps), min(count, count - steps))
    return lax.ppermute(value, axis, [(source, source + steps) for source in range(first, last)])


def local(
    queries,
    keys,
    values,
    doc_ids,
    sink_logits,
    out_weight,
    residual,
    norm_gain,
    routes,
    route_weights,
    gate_weight,
    up_weight,
    down_weight,
):
    span_rows = queries.shape[0]
    kv_width = keys.shape[1]
    kv_groups = kv_width // HEAD_DIM
    heads_here = queries.shape[1] // HEAD_DIM
    group_ratio = heads_here // kv_groups
    reach_back = WINDOW - 1
    score_scale = 1.0 / math.sqrt(HEAD_DIM)
    doc_float = (doc_ids + 1).astype(jnp.float32)
    key_value = jnp.concatenate([keys, values], axis=1).astype(jnp.float32)
    tail_pairs, tail_docs = (
        passed_along(key_value[span_rows - reach_back :].astype(jnp.bfloat16), "sp", 1).astype(
            jnp.float32
        ),
        passed_along(doc_float[span_rows - reach_back :].astype(jnp.bfloat16), "sp", 1).astype(
            jnp.float32
        ),
    )
    all_keys = jnp.concatenate([tail_pairs[:, :kv_width].astype(jnp.bfloat16), keys], axis=0)
    all_values = jnp.concatenate([tail_pairs[:, kv_width:].astype(jnp.bfloat16), values], axis=0)
    all_docs = jnp.concatenate([tail_docs, doc_float], axis=0)
    block_rows = min(512, span_rows)
    sink_table = sink_logits.reshape(kv_groups, group_ratio, 1)
    offsets = (
        jnp.arange(block_rows)[:, None] + reach_back - jnp.arange(block_rows + reach_back)[None, :]
    )
    window_mask = (offsets >= 0) & (offsets <= reach_back)
    pieces = []
    for block_index in range(span_rows // block_rows):
        first_row = block_index * block_rows
        query_rows = queries[first_row : first_row + block_rows].reshape(
            block_rows, kv_groups, group_ratio, HEAD_DIM
        )
        key_rows = all_keys[first_row : first_row + block_rows + reach_back].reshape(
            block_rows + reach_back, kv_groups, HEAD_DIM
        )
        value_rows = all_values[first_row : first_row + block_rows + reach_back].reshape(
            block_rows + reach_back, kv_groups, HEAD_DIM
        )
        scores = (
            jnp.einsum("bgrd,sgd->grbs", query_rows, key_rows, preferred_element_type=jnp.float32)
            * score_scale
        )
        same_doc = (
            doc_float[first_row : first_row + block_rows][:, None]
            == all_docs[first_row : first_row + block_rows + reach_back][None, :]
        )
        scores = jnp.where(window_mask & same_doc, scores, masked_score)
        row_max = jnp.maximum(scores.max(-1), sink_table)
        exp_scores = jnp.exp(scores - row_max[..., None])
        denominator = exp_scores.sum(-1) + jnp.exp(sink_table - row_max)
        weighted = jnp.einsum(
            "grbs,sgd->bgrd",
            exp_scores.astype(jnp.bfloat16),
            value_rows,
            preferred_element_type=jnp.float32,
        )
        weighted = weighted / jnp.transpose(denominator, (2, 0, 1))[..., None]
        pieces.append(weighted.astype(jnp.bfloat16).reshape(block_rows, heads_here * HEAD_DIM))
    attended = jnp.concatenate(pieces, axis=0)
    rows_here = attended
    projected = lax.psum_scatter(
        jnp.dot(rows_here, out_weight, preferred_element_type=jnp.float32).astype(jnp.bfloat16),
        "tp",
        scatter_dimension=0,
        tiled=True,
    ).astype(jnp.float32)
    stream = residual.astype(jnp.float32) + projected
    mean_value = stream.mean(-1, keepdims=True)
    centred = stream - mean_value
    variance = (centred * centred).mean(-1, keepdims=True)
    normed = (centred * lax.rsqrt(variance + layer_epsilon) * norm_gain).astype(jnp.bfloat16)
    token_count = residual.shape[0]
    width = residual.shape[1]
    route_count = routes.shape[1]
    expert_count = lax.axis_size("sp") * gate_weight.shape[0]
    capacity = 9 * route_count * token_count // (8 * expert_count)
    flat_routes = routes.reshape(-1)
    one_hot = (flat_routes[:, None] == jnp.arange(expert_count)[None, :]).astype(jnp.int32)
    slot_ids = jnp.sum((jnp.cumsum(one_hot, axis=0) - 1) * one_hot, axis=1)
    destination = flat_routes * capacity + slot_ids
    slot_range = jnp.arange(expert_count * capacity)
    selector = jnp.any(
        slot_range[:, None, None] == destination.reshape(token_count, route_count)[None], axis=2
    )
    dispatch = jnp.dot(
        selector.astype(jnp.bfloat16), normed, preferred_element_type=jnp.float32
    ).astype(jnp.bfloat16)
    inbound = lax.all_to_all(
        dispatch.reshape(expert_count, capacity, width),
        "sp",
        split_axis=0,
        concat_axis=0,
        tiled=True,
    )
    arrived = inbound.reshape(-1, width)
    row_piece = lax.all_gather(arrived, "tp", axis=0, tiled=True)
    gate = jnp.dot(row_piece, gate_weight[0], preferred_element_type=jnp.float32)
    upward = jnp.dot(row_piece, up_weight[0], preferred_element_type=jnp.float32)
    hidden = (jax.nn.silu(gate) * upward).astype(jnp.bfloat16)
    rows_here = hidden
    partial_value = jnp.dot(rows_here, down_weight[0], preferred_element_type=jnp.float32).astype(
        jnp.bfloat16
    )
    returned = lax.psum_scatter(
        lax.optimization_barrier(partial_value).astype(jnp.float32).astype(jnp.bfloat16),
        "tp",
        scatter_dimension=0,
        tiled=True,
    )
    back_rows = lax.all_to_all(
        returned.reshape(inbound.shape), "sp", split_axis=0, concat_axis=0, tiled=True
    ).reshape(-1, width)
    picked = back_rows[destination].astype(jnp.float32).reshape(token_count, route_count, width)
    combined = jnp.sum(picked * route_weights[..., None], axis=1)
    return (stream + combined).astype(jnp.bfloat16)


def solution(mesh):
    placed = (
        P("sp", "tp"),
        P("sp", "tp"),
        P("sp", "tp"),
        P("sp"),
        P("tp"),
        P("tp", None),
        P(("sp", "tp"), None),
        P(),
        P(("sp", "tp"), None),
        P(("sp", "tp"), None),
        P("sp", None, "tp"),
        P("sp", None, "tp"),
        P("sp", "tp", None),
    )
    return jax.shard_map(
        local, mesh=mesh, in_specs=placed, out_specs=P(("sp", "tp"), None), check_vma=False
    )
```

profile of v0, /device:TPU:0, one launch (start us, length us, event | category | flops | bytes accessed | tf_op | source)
XLA Modules:
  0.0 232.7 jit_solution(13959658188333084272)
XLA Ops:
  7.4 4.9 %collective-permute-start.1 = (bf16[127]{0:T(256)(128)(2,1)S(1)}, bf16[127]{0:T(256)(128)(2,1)S(1)}, u32[]{:S(2)}, u32[]{:S(2)}) collective-permute-start(bf16[127]{0:T(256)(128)(2,1)S(1)} %slice.18), channel_id=1, source_target_pairs={{0,8},{8,16},{16,24},{1,9},{9,17},{17,25},{2,10},{10,18},{18,26},{... | collective-permute-start | bytes 770 | tf_op jit(solution)/shard_map/ppermute | solution.py:19
  13.1 3.4 %collective-permute-start = (bf16[127,256]{1,0:T(8,128)(2,1)S(1)}, bf16[127,256]{1,0:T(8,128)(2,1)S(1)}, u32[]{:S(2)}, u32[]{:S(2)}) collective-permute-start(bf16[127,256]{1,0:T(8,128)(2,1)S(1)} %pad_maximum_fusion.2), channel_id=1, source_target_pairs={{0,8},{8,16},{16,24},{1,9},{9,17},{17,25},{2,10},{10,18},{18,26},{... | collective-permute-start | bytes 195080 | tf_op jit(solution)/shard_map/ppermute | solution.py:19
  16.5 1.1 copy.30
  18.9 1.0 pad_maximum_fusion
  20.1 1.1 fusion.2
  21.3 2.2 copy-done.1
  23.5 1.1 fusion
  24.9 4.0 %fusion.23 = bf16[512,2,2,64]{0,3,2,1:T(8,128)(2,1)S(1)} fusion(bf16[639,2,64,1]{0,2,3,1:T(8,128)(2,1)S(1)} %bitcast.63, f32[2,639,512,2]{2,1,3,0:T(8,128)} %copy-done.1, f32[2,2,512]{2,1,0:T(2,128)S(1)} %broadcast_maximum_fusion, pred[512,639]{0,1:T(8,128)(4,1)S(1)} %fusion.16, f32[512,2,2]{0,2,1:T(2,128)S(1)} %add_bitcast_fusion), kind=kOutput, calls=%fused_computation.25 | convolution fusion | flops 173006848 | bytes 6003968 | tf_op jit(solution)/shard_map/grbs,sgd->bgrd/dot_general | solution.py:87
  28.9 2.1 convolution_convert_fusion.1
  32.1 36.7 %reduce-scatter.3.cloned.1.call-done = bf16[64,2048]{1,0:T(8,128)(2,1)} async-done(((bf16[512,2048]{1,0:T(8,128)(2,1)}), bf16[64,2048]{1,0:T(8,128)(2,1)}) %reduce-scatter.3.cloned.1.call-update) | async-done | bytes 262160 | tf_op jit(solution)/shard_map/reduce_scatter | solution.py:97
  68.8 1.1 fusion.26
  70.0 1.2 multiply_reduce_fusion.1
  71.2 1.3 convolution_convert_fusion.2
  72.7 11.1 %all_to_all.10 = bf16[4,36,2048]{2,1,0:T(8,128)(2,1)S(1)} all-to-all(bf16[4,36,2048]{2,1,0:T(8,128)(2,1)S(1)} %reshape.95), channel_id=1, replica_groups=mesh['sp'=4,'tp'=8] {'sp'}, dimensions={0} | all-to-all | bytes 1179648 | tf_op jit(solution)/shard_map/all_to_all | solution.py:124
  83.8 1.0 reshape.96
  85.0 49.7 %all-gather.2.cloned.1.call-done = bf16[1152,2048]{1,0:T(8,128)(2,1)} async-done(((bf16[144,2048]{1,0:T(8,128)(2,1)}), bf16[1152,2048]{1,0:T(8,128)(2,1)}) %all-gather.2.cloned.1.call-update) | async-done | bytes 4718608 | tf_op jit(solution)/shard_map/all_gather | solution.py:132
  134.7 8.1 %fusion.5 = f32[1152,896]{1,0:T(8,128)S(1)} fusion(bf16[1152,2048]{1,0:T(8,128)(2,1)} %all-gather.2.cloned.1.call-done, bf16[1,2048,896]{2,1,0:T(8,128)(2,1)} %param.23), kind=kOutput, calls=%fused_computation.10 | convolution fusion | flops 4227858432 | bytes 12517376 | tf_op jit(solution)/shard_map/dot_general | solution.py:133
  142.8 5.3 %fusion.7 = bf16[1152,896]{1,0:T(8,128)(2,1)S(1)} fusion(bf16[1152,2048]{1,0:T(8,128)(2,1)S(1)} %copy-done.7, bf16[1,2048,896]{2,1,0:T(8,128)(2,1)S(1)} %copy-done.8, f32[1152,896]{1,0:T(8,128)S(1)} %fusion.5), kind=kOutput, calls=%fused_computation.12 | convolution fusion | flops 4234051584 | bytes 14581760 | tf_op jit(solution)/shard_map/dot_general | solution.py:134
  148.2 6.7 %convolution_convert_fusion = bf16[1152,2048]{1,0:T(8,128)(2,1)} fusion(bf16[1152,896]{1,0:T(8,128)(2,1)S(1)} %fusion.7, bf16[1,896,2048]{2,1,0:T(8,128)(2,1)S(1)} %copy-done.9), kind=kOutput, calls=%fused_computation.1 | convolution fusion | flops 4230217728 | bytes 10452992 | tf_op jit(solution)/shard_map/dot_general | solution.py:137
  154.9 53.8 %reduce-scatter.5.cloned.1.call-done = bf16[144,2048]{1,0:T(8,128)(2,1)} async-done(((bf16[1152,2048]{1,0:T(8,128)(2,1)}), bf16[144,2048]{1,0:T(8,128)(2,1)}) %reduce-scatter.5.cloned.1.call-update) | async-done | bytes 589840 | tf_op jit(solution)/shard_map/reduce_scatter | solution.py:140
  208.7 2.0 reshape.97
  210.7 3.6 %all-to-all-start.1 = ((bf16[4,36,2048]{2,1,0:T(8,128)(2,1)}), bf16[4,36,2048]{2,1,0:T(8,128)(2,1)S(1)}, u32[]{:S(2)}, u32[]{:S(2)}) async-start(bf16[4,36,2048]{2,1,0:T(8,128)(2,1)} %reshape.97), calls=%async_computation.3 | async-start | bytes 1310720 | tf_op jit(solution)/shard_map/all_to_all | solution.py:146
  214.6 7.4 %all-to-all-done.1 = bf16[4,36,2048]{2,1,0:T(8,128)(2,1)S(1)} async-done(((bf16[4,36,2048]{2,1,0:T(8,128)(2,1)}), bf16[4,36,2048]{2,1,0:T(8,128)(2,1)S(1)}, u32[]{:S(2)}, u32[]{:S(2)}) %all-to-all-start.1) | async-done | bytes 589856 | tf_op jit(solution)/shard_map/all_to_all | solution.py:146
  223.8 1.5 multiply_reduce_fusion
  (60 shorter events, 7.6 us)
Async XLA Ops:
  6.5 22.4 %copy-start = (bf16[256,2048]{1,0:T(8,128)(2,1)S(1)}, bf16[256,2048]{1,0:T(8,128)(2,1)}, u32[]{:S(2)}) copy-start(bf16[256,2048]{1,0:T(8,128)(2,1)} %param.18) | copy-start | bytes 3145732
  6.5 62.3 %reduce-scatter.3.cloned.1.call-start = ((), (), s32[]{:S(2)}) async-start(), calls=%async_computation.4 | async-start | bytes 2359296 | tf_op jit(solution)/shard_map/reduce_scatter | solution.py:97
  7.4 10.9 %collective-permute-start.1 = (bf16[127]{0:T(256)(128)(2,1)S(1)}, bf16[127]{0:T(256)(128)(2,1)S(1)}, u32[]{:S(2)}, u32[]{:S(2)}) collective-permute-start(bf16[127]{0:T(256)(128)(2,1)S(1)} %slice.18), channel_id=1, source_target_pairs={{0,8},{8,16},{16,24},{1,9},{9,17},{17,25},{2,10},{10,18},{18,26},{... | collective-permute-start | bytes 770 | tf_op jit(solution)/shard_map/ppermute | solution.py:19
  13.1 5.8 %collective-permute-start = (bf16[127,256]{1,0:T(8,128)(2,1)S(1)}, bf16[127,256]{1,0:T(8,128)(2,1)S(1)}, u32[]{:S(2)}, u32[]{:S(2)}) collective-permute-start(bf16[127,256]{1,0:T(8,128)(2,1)S(1)} %pad_maximum_fusion.2), channel_id=1, source_target_pairs={{0,8},{8,16},{16,24},{1,9},{9,17},{17,25},{2,10},{10,18},{18,26},{... | collective-permute-start | bytes 195080 | tf_op jit(solution)/shard_map/ppermute | solution.py:19
  21.2 2.3 copy-start.1
  28.9 2.2 copy-start.5
  28.9 40.0 %copy-start.2 = (bf16[64,2048]{1,0:T(8,128)(2,1)S(1)}, bf16[64,2048]{1,0:T(8,128)(2,1)}, u32[]{:S(2)}) copy-start(bf16[64,2048]{1,0:T(8,128)(2,1)} %param.19) | copy-start | bytes 786436
  28.9 42.3 %copy-start.4 = (f32[2048]{0:T(1024)S(1)}, f32[2048]{0:T(1024)}, u32[]{:S(2)}) copy-start(f32[2048]{0:T(1024)} %param.20) | copy-start | bytes 24580
  31.0 103.7 %all-gather.2.cloned.1.call-start = ((), (), s32[]{:S(2)}) async-start(), calls=%async_computation.5 | async-start | bytes 5308416 | tf_op jit(solution)/shard_map/all_gather | solution.py:132
  84.7 124.0 %reduce-scatter.5.cloned.1.call-start = ((), (), s32[]{:S(2)}) async-start(), calls=%async_computation.6 | async-start | bytes 5308416 | tf_op jit(solution)/shard_map/reduce_scatter | solution.py:140
  134.7 8.1 %copy-start.7 = (bf16[1152,2048]{1,0:T(8,128)(2,1)S(1)}, bf16[1152,2048]{1,0:T(8,128)(2,1)}, u32[]{:S(2)}) copy-start(bf16[1152,2048]{1,0:T(8,128)(2,1)} %all-gather.2.cloned.1.call-done) | copy-start | bytes 14155780
  134.7 8.1 %copy-start.8 = (bf16[1,2048,896]{2,1,0:T(8,128)(2,1)S(1)}, bf16[1,2048,896]{2,1,0:T(8,128)(2,1)}, u32[]{:S(2)}) copy-start(bf16[1,2048,896]{2,1,0:T(8,128)(2,1)} %param.24) | copy-start | bytes 11010052
  142.8 5.3 %copy-start.9 = (bf16[1,896,2048]{2,1,0:T(8,128)(2,1)S(1)}, bf16[1,896,2048]{2,1,0:T(8,128)(2,1)}, u32[]{:S(2)}) copy-start(bf16[1,896,2048]{2,1,0:T(8,128)(2,1)} %param.25) | copy-start | bytes 11010052
  154.9 59.6 %copy-start.6 = (f32[64,2]{0,1:T(2,128)S(1)}, f32[64,2]{0,1:T(2,128)}, u32[]{:S(2)}) copy-start(f32[64,2]{0,1:T(2,128)} %param.22) | copy-start | bytes 1540
  210.7 11.3 %all-to-all-start.1 = ((bf16[4,36,2048]{2,1,0:T(8,128)(2,1)}), bf16[4,36,2048]{2,1,0:T(8,128)(2,1)S(1)}, u32[]{:S(2)}, u32[]{:S(2)}) async-start(bf16[4,36,2048]{2,1,0:T(8,128)(2,1)} %reshape.97), calls=%async_computation.3 | async-start | bytes 1310720 | tf_op jit(solution)/shard_map/all_to_all | solution.py:146
  222.2 3.2 %copy-start.3 = (bf16[64,2048]{1,0:T(8,128)(2,1)S(1)}, bf16[64,2048]{1,0:T(8,128)(2,1)}, u32[]{:S(2)}) copy-start(bf16[64,2048]{1,0:T(8,128)(2,1)} %reduce-scatter.3.cloned.1.call-done) | copy-start | bytes 786436
Sparse Core Ops, SparseCore 0:
  31.1 37.6 reduce-scatter.2
  84.9 49.7 all-gather.1
  155.0 53.6 reduce-scatter.4
where the time goes:
time: 233 us
  waiting for transfers between devices  148 us (64%)
  matrix products  28.7 us (12%)
  between operations  13.4 us (6%)
  starting transfers between devices  12.2 us (5%)
  blocking collectives  11.1 us (5%)
  local copies, waits for them, and re-layouts  9.98 us (4%)
  other arithmetic  9.64 us (4%)
    reduce_scatter x1, waiting for transfers between devices, local(): lax.psum_scatter(lax.optimization_barrier(partial_value).astype(jnp.float...  53.8 us
    all_gather x1, waiting for transfers between devices, local(): row_piece = lax.all_gather(arrived, 'tp', axis=0, tiled=True)  49.7 us
    reduce_scatter x1, waiting for transfers between devices, local(): lax.psum_scatter(jnp.dot(rows_here, out_weight, preferred_element_type=jn...  36.7 us
    all_to_all x1, blocking collectives, local(): lax.all_to_all(dispatch.reshape(expert_count, capacity, width), 'sp', spl...  11.1 us
    ppermute x2, starting transfers between devices, passed_along(): lax.ppermute(value, axis, [(source, source + steps) for source in range(f...  8.26 us
    dot_general x1, matrix products, local(): jnp.dot(row_piece, gate_weight[0], preferred_element_type=jnp.float32)  8.11 us
    all_to_all x1, waiting for transfers between devices, local(): lax.all_to_all(returned.reshape(inbound.shape), 'sp', split_axis=0, conca...  7.42 us
    dot_general x1, matrix products, local(): jnp.dot(rows_here, down_weight[0], preferred_element_type=jnp.float32)  6.73 us
  transfers between devices with their start and end apart: 6, of which 4 were waited for; matrix products, arithmetic and copies ran while one was open for 2% of the time, Pallas kernels for 0%

commit v1 on v0

v1 whole, which is shorter than its diff:
```python
import math

import jax
import jax.numpy as jnp
from jax import lax
from jax.experimental import pallas as pl
from jax.experimental.layout import Layout, with_layout_constraint
from jax.experimental.pallas import tpu as pltpu
from jax.sharding import PartitionSpec as P


HEAD_DIM = 64
WINDOW = 128
CORES = 2
CHUNKS = 2

layer_epsilon = 1e-05
masked_score = -1e30


def passed_along(value, axis, steps):
    count = lax.axis_size(axis)
    first, last = (max(0, -steps), min(count, count - steps))
    return lax.ppermute(value, axis, [(source, source + steps) for source in range(first, last)])


def z_shift(value, steps):
    count = lax.axis_size("tp")
    return lax.ppermute(
        value, "tp", [(source, (source + CORES * steps) % count) for source in range(count)]
    )


def swap_cores(value):
    return lax.ppermute(value, "tp", [(source, source ^ 1) for source in range(lax.axis_size("tp"))])


def sp_exchange(value, flip):
    return lax.ppermute(value, "sp", [(source, source ^ flip) for source in range(lax.axis_size("sp"))])


def row_major(value):
    return with_layout_constraint(value, Layout(major_to_minor=tuple(range(value.ndim))))


def attend_kernel(sink_ref, query_ref, key_ref, value_ref, query_doc_ref, key_doc_ref, out_ref):
    heads_here = query_ref.shape[1] // HEAD_DIM
    group_ratio = query_ref.shape[1] // key_ref.shape[1]
    score_scale = 1.0 / math.sqrt(HEAD_DIM)
    offsets = (
        lax.broadcasted_iota(jnp.int32, (WINDOW, 2 * WINDOW), 0)
        + WINDOW
        - lax.broadcasted_iota(jnp.int32, (WINDOW, 2 * WINDOW), 1)
    )
    window_mask = (offsets >= 0) & (offsets < WINDOW)
    for block in range(query_ref.shape[0] // WINDOW):
        rows = pl.ds(block * WINDOW, WINDOW)
        reach = pl.ds(block * WINDOW, 2 * WINDOW)
        allowed = window_mask & (query_doc_ref[rows, :] == key_doc_ref[:, reach])
        pieces = []
        for head in range(heads_here):
            group = head // group_ratio
            columns = pl.ds(group * HEAD_DIM, HEAD_DIM)
            scores = lax.dot_general(
                query_ref[rows, pl.ds(head * HEAD_DIM, HEAD_DIM)],
                key_ref[reach, columns],
                (((1,), (1,)), ((), ())),
                preferred_element_type=jnp.float32,
            )
            scores = jnp.where(allowed, scores * score_scale, masked_score)
            sink = sink_ref[head]
            row_max = jnp.maximum(scores.max(-1, keepdims=True), sink)
            exp_scores = jnp.exp(scores - row_max)
            denominator = exp_scores.sum(-1, keepdims=True) + jnp.exp(sink - row_max)
            weighted = jnp.dot(
                exp_scores.astype(jnp.bfloat16),
                value_ref[reach, columns],
                preferred_element_type=jnp.float32,
            )
            pieces.append((weighted / denominator).astype(jnp.bfloat16))
        out_ref[rows, :] = jnp.concatenate(pieces, axis=1)


def attention(queries, keys, values, doc_ids, sink_logits):
    span_rows = queries.shape[0]
    kv_width = keys.shape[1]
    doc_float = (doc_ids + 1).astype(jnp.float32)
    doc_row = jnp.pad(doc_float[span_rows - WINDOW :], (0, 2 * kv_width - WINDOW))
    doc_rows = jnp.broadcast_to(doc_row.astype(jnp.bfloat16), (16, 2 * kv_width))
    tail = jnp.concatenate(
        [
            jnp.concatenate(
                [keys[span_rows - WINDOW :], values[span_rows - WINDOW :]], axis=1
            ),
            doc_rows,
        ],
        axis=0,
    )
    tail = passed_along(tail, "sp", 1)
    all_keys = jnp.concatenate([tail[:WINDOW, :kv_width], keys], axis=0)
    all_values = jnp.concatenate([tail[:WINDOW, kv_width:], values], axis=0)
    all_docs = jnp.concatenate([tail[WINDOW, :WINDOW].astype(jnp.float32), doc_float], axis=0)
    vmem = pl.BlockSpec(memory_space=pltpu.VMEM)
    return pl.pallas_call(
        attend_kernel,
        out_shape=jax.ShapeDtypeStruct(queries.shape, jnp.bfloat16),
        in_specs=[pl.BlockSpec(memory_space=pltpu.SMEM)] + [vmem] * 5,
        out_specs=vmem,
        name="attend",
    )(sink_logits, queries, all_keys, all_values, doc_float[:, None], all_docs[None, :])


def layer(
    queries,
    keys,
    values,
    doc_ids,
    sink_logits,
    out_weight,
    residual,
    norm_gain,
    routes,
    route_weights,
    gate_weight,
    up_weight,
    down_weight,
):
    tokens, width = residual.shape
    planes = lax.axis_size("tp") // CORES
    columns = lax.axis_size("sp")
    place = lax.axis_index("tp")
    plane, core = place // CORES, place % CORES
    column = lax.axis_index("sp")
    route_count = routes.shape[1]
    expert_count = columns * gate_weight.shape[0]
    capacity = 9 * route_count * tokens // (8 * expert_count)

    flat_routes = routes.reshape(-1)
    one_hot = (flat_routes[:, None] == jnp.arange(expert_count)[None, :]).astype(jnp.float32)
    order = jnp.arange(flat_routes.shape[0])
    before = (order[:, None] > order[None, :]).astype(jnp.float32)
    slot_ids = jnp.sum(jnp.dot(before, one_hot) * one_hot, axis=1).reshape(routes.shape)
    upper = route_weights.astype(jnp.bfloat16)
    lower = (route_weights - upper.astype(jnp.float32)).astype(jnp.bfloat16)
    table = jnp.concatenate(
        [routes.astype(jnp.bfloat16), slot_ids.astype(jnp.bfloat16), upper, lower], axis=1
    )
    table = jnp.pad(table, ((0, 0), (0, 128 - table.shape[1])))

    attended = attention(queries, keys, values, doc_ids, sink_logits)
    attended = attended.reshape(planes, CORES, tokens, -1)
    attended = jnp.concatenate([attended, attended[:, :1]], axis=1)
    attended = lax.dynamic_slice_in_dim(attended, core, CORES, 1)
    attended = jnp.concatenate([attended, attended[: planes - 1]], axis=0)
    attended = lax.dynamic_slice_in_dim(attended, plane, planes, 0)

    def project(which):
        return jnp.dot(
            attended[:, which].reshape(planes * tokens, -1),
            out_weight,
            preferred_element_type=jnp.float32,
        )

    theirs = row_major(swap_cores(row_major(project(1).astype(jnp.bfloat16))))
    summed = project(0) + theirs.astype(jnp.float32)
    outgoing = row_major(summed.astype(jnp.bfloat16))
    stream = residual.astype(jnp.float32) + summed[:tokens]
    sent = [
        row_major(z_shift(row_major(outgoing[step * tokens : (step + 1) * tokens]), step))
        for step in range(1, planes)
    ]
    for piece in sent:
        stream = stream + piece.astype(jnp.float32)
    mean_value = stream.mean(-1, keepdims=True)
    centred = stream - mean_value
    variance = (centred * centred).mean(-1, keepdims=True)
    normed = (centred * lax.rsqrt(variance + layer_epsilon) * norm_gain).astype(jnp.bfloat16)
    packet = jnp.concatenate([normed, table], axis=1)
    packets = [packet] + [z_shift(packet, step) for step in range(1, planes)]

    combined = stream
    chunks = CHUNKS if planes % CHUNKS == 0 else 1
    per_chunk = planes // chunks
    slots = per_chunk * capacity
    slot_range = jnp.arange(expert_count * slots)
    for chunk in range(chunks):
        held = jnp.concatenate(packets[chunk * per_chunk : (chunk + 1) * per_chunk], axis=0)
        entry = held[:, width:].astype(jnp.float32)
        expert = entry[:, :route_count].astype(jnp.int32)
        slot = entry[:, route_count : 2 * route_count].astype(jnp.int32)
        local_plane = jnp.arange(per_chunk * tokens)[:, None] // tokens
        hits = [
            (
                ((expert ^ column) * slots + local_plane * capacity + slot)[:, k : k + 1]
                == slot_range[None, :]
            )
            for k in range(route_count)
        ]
        selector = sum(hit.astype(jnp.float32) for hit in hits).astype(jnp.bfloat16)

        def mixer(first):
            return sum(
                jnp.where(hit, entry[:, first + k : first + k + 1], 0.0)
                for k, hit in enumerate(hits)
            ).astype(jnp.bfloat16)

        mixers = mixer(2 * route_count), mixer(3 * route_count)
        dispatch = lax.dot_general(
            selector,
            held[:, :width],
            (((0,), (0,)), ((), ())),
            preferred_element_type=jnp.float32,
        ).astype(jnp.bfloat16)
        arrived = [dispatch[:slots]] + [
            sp_exchange(dispatch[flip * slots : (flip + 1) * slots], flip)
            for flip in range(1, columns)
        ]
        arrived = jnp.concatenate(arrived, axis=0)
        rows = jnp.concatenate([arrived, swap_cores(arrived)], axis=0)
        half = arrived.shape[0]
        gate = jnp.dot(rows, gate_weight[0], preferred_element_type=jnp.float32)
        upward = jnp.dot(rows, up_weight[0], preferred_element_type=jnp.float32)
        hidden = (jax.nn.silu(gate) * upward).astype(jnp.bfloat16)
        outcome = jnp.dot(hidden, down_weight[0], preferred_element_type=jnp.float32).astype(
            jnp.bfloat16
        )
        other = swap_cores(outcome[half:])
        total = (outcome[:half].astype(jnp.float32) + other.astype(jnp.float32)).astype(
            jnp.bfloat16
        )
        back = [total[:slots]] + [
            sp_exchange(total[flip * slots : (flip + 1) * slots], flip)
            for flip in range(1, columns)
        ]
        back = jnp.concatenate(back, axis=0)
        share = jnp.dot(mixers[0], back, preferred_element_type=jnp.float32) + jnp.dot(
            mixers[1], back, preferred_element_type=jnp.float32
        )
        for local_index in range(per_chunk):
            step = chunk * per_chunk + local_index
            piece = share[local_index * tokens : (local_index + 1) * tokens]
            if step:
                piece = row_major(z_shift(row_major(piece.astype(jnp.bfloat16)), -step))
                piece = piece.astype(jnp.float32)
            combined = combined + piece
    return combined.astype(jnp.bfloat16)


def solution(mesh):
    placed = (
        P("sp", "tp"),
        P("sp", "tp"),
        P("sp", "tp"),
        P("sp"),
        P("tp"),
        P("tp", None),
        P(("sp", "tp"), None),
        P(),
        P(("sp", "tp"), None),
        P(("sp", "tp"), None),
        P("sp", None, "tp"),
        P("sp", None, "tp"),
        P("sp", "tp", None),
    )
    return jax.shard_map(
        layer, mesh=mesh, in_specs=placed, out_specs=P(("sp", "tp"), None), check_vma=False
    )
```

time: 233 us -> 198 us (0.85)
  waiting for transfers between devices: 148 us -> 78.7 us
  starting transfers between devices: 12.2 us -> 50.7 us
  between operations: 13.4 us -> 0.49 us
  blocking collectives: 11.1 us -> 0 us
  matrix products: 28.7 us -> 37.8 us
  local copies, waits for them, and re-layouts: 9.98 us -> 16.8 us
  Pallas kernels: 0 us -> 4.14 us
    reduce_scatter x2 -> x0, waiting for transfers between devices: 90.5 us -> none  [the longest x1 53.8 us: local(): lax.psum_scatter(lax.optimization_barrier(partial_value).astype(jnp.float...]
    ppermute x0 -> x26, waiting for transfers between devices: none -> 77.7 us  [the longest x9 46.8 us: z_shift(): lax.ppermute(value, 'tp', [(source, (source + CORES * steps) % count) for...]
    all_gather x1 -> x0, waiting for transfers between devices: 49.7 us -> none  [local(): row_piece = lax.all_gather(arrived, 'tp', axis=0, tiled=True)]
    ppermute x0 -> x26, starting transfers between devices: none -> 45.8 us  [the longest x9 27.1 us: z_shift(): lax.ppermute(value, 'tp', [(source, (source + CORES * steps) % count) for...]
    all_to_all x1 -> x0, blocking collectives: 11.1 us -> none  [local(): lax.all_to_all(dispatch.reshape(expert_count, capacity, width), 'sp', spl...]
    dot_general x7 -> x13, matrix products: 28.7 us -> 37.8 us  [the longest x2 22.2 us: layer(): jnp.dot(hidden, down_weight[0], preferred_element_type=jnp.float32)]
    slice x2 -> x20, local copies, waits for them, and re-layouts: 0.08 us -> 8.02 us  [the longest x2 4.08 us: layer(): other = swap_cores(outcome[half:])]
    all_to_all x1 -> x0, waiting for transfers between devices: 7.42 us -> none  [local(): lax.all_to_all(returned.reshape(inbound.shape), 'sp', split_axis=0, conca...]
  transfers between devices with their start and end apart: 6 -> 27, of which waited for: 4 -> 17; matrix products, arithmetic and copies ran while one was open for 2% -> 23% of each run, Pallas kernels for 0% -> 0%
where the time goes in v1:
time: 198 us; the launch traced here: 197 us
  waiting for transfers between devices  78.7 us (40%)
  starting transfers between devices  50.7 us (26%)
  matrix products  37.8 us (19%)
  local copies, waits for them, and re-layouts  16.8 us (8%)
  other arithmetic  8.58 us (4%)
  Pallas kernels  4.14 us (2%)
    ppermute x9, waiting for transfers between devices, z_shift(): lax.ppermute(value, 'tp', [(source, (source + CORES * steps) % count) for...  46.8 us
    ppermute x12, waiting for transfers between devices, sp_exchange(): lax.ppermute(value, 'sp', [(source, source ^ flip) for source in range(la...  28.2 us
    ppermute x9, starting transfers between devices, z_shift(): lax.ppermute(value, 'tp', [(source, (source + CORES * steps) % count) for...  27.1 us
    dot_general x2, matrix products, layer(): jnp.dot(hidden, down_weight[0], preferred_element_type=jnp.float32)  22.2 us
    ppermute x12, starting transfers between devices, sp_exchange(): lax.ppermute(value, 'sp', [(source, source ^ flip) for source in range(la...  18.1 us
    dot_general x2, matrix products, layer(): upward = jnp.dot(rows, up_weight[0], preferred_element_type=jnp.float32)  9.97 us
    unnamed x32, local copies, waits for them, and re-layouts  5.18 us
    ppermute x1, starting transfers between devices, passed_along(): lax.ppermute(value, axis, [(source, source + steps) for source in range(f...  4.87 us
  transfers between devices with their start and end apart: 27, of which 17 were waited for; matrix products, arithmetic and copies ran while one was open for 23% of the time, Pallas kernels for 0%

profile of v1, /device:TPU:0, one launch (start us, length us, event | category | flops | bytes accessed | tf_op | source)
XLA Modules:
  0.0 197.2 jit_solution(10722348624338012193)
XLA Ops:
  2.3 4.9 %collective-permute-start = (bf16[144,256]{1,0:T(8,128)(2,1)S(1)}, bf16[144,256]{1,0:T(8,128)(2,1)S(1)}, u32[]{:S(2)}, u32[]{:S(2)}) collective-permute-start(bf16[144,256]{1,0:T(8,128)(2,1)S(1)} %pad_maximum_fusion.15), channel_id=1, source_target_pairs={{0,8},{8,16},{16,24},{1,9},{9,17},{17,25},{2,10},{10,18},{18,26},{... | collective-permute-start | bytes 221192 | tf_op jit(solution)/shard_map/ppermute | solution.py:24
  11.5 4.1 %attend.1 = bf16[512,256]{1,0:T(8,128)(2,1)} custom-call(f32[4]{0:T(128)} %sink_ref.1, bf16[512,256]{1,0:T(8,128)(2,1)} %query_ref.1, bf16[640,128]{1,0:T(8,128)(2,1)} %get-tuple-element.54.key_ref, bf16[640,128]{1,0:T(8,128)(2,1)} %get-tuple-element.55.value_ref, f32[512,1]{1,0:T(8,128)} %copy.32.query_doc_ref, f32[1,640]{1,0:T(1,128)} %broadcast_in_dim.93.key_doc_ref), custom_call_target="tpu_custom_call" | custom-call | tf_op jit(solution)/shard_map/attend/pallas_call | solution.py:104
  18.3 2.6 %collective-permute-done.1 = bf16[256,2048]{1,0:T(8,128)(2,1)S(1)} collective-permute-done((bf16[256,2048]{1,0:T(8,128)(2,1)S(1)}, bf16[256,2048]{1,0:T(8,128)(2,1)S(1)}, u32[]{:S(2)}, u32[]{:S(2)}) %collective-permute-start.1) | collective-permute-done | bytes 1048608 | tf_op jit(solution)/shard_map/ppermute | solution.py:35
  24.4 2.6 %collective-permute-start.3 = (bf16[64,2048]{1,0:T(8,128)(2,1)S(1)}, bf16[64,2048]{1,0:T(8,128)(2,1)S(1)}, u32[]{:S(2)}, u32[]{:S(2)}) collective-permute-start(bf16[64,2048]{1,0:T(8,128)(2,1)S(1)} %get-tuple-element.42), channel_id=1, source_target_pairs={{0,4},{1,5},{2,6},{3,7},{4,0},{5,1},{6,2},{7,3},{8,12},{9,13},{10,... | collective-permute-start | bytes 786440 | tf_op jit(solution)/shard_map/ppermute | solution.py:29
  29.4 4.6 %collective-permute-done.2 = bf16[64,2048]{1,0:T(8,128)(2,1)S(1)} collective-permute-done((bf16[64,2048]{1,0:T(8,128)(2,1)S(1)}, bf16[64,2048]{1,0:T(8,128)(2,1)S(1)}, u32[]{:S(2)}, u32[]{:S(2)}) %collective-permute-start.2) | collective-permute-done | bytes 262176 | tf_op jit(solution)/shard_map/ppermute | solution.py:29
  34.0 10.5 %collective-permute-done.3 = bf16[64,2048]{1,0:T(8,128)(2,1)S(1)} collective-permute-done((bf16[64,2048]{1,0:T(8,128)(2,1)S(1)}, bf16[64,2048]{1,0:T(8,128)(2,1)S(1)}, u32[]{:S(2)}, u32[]{:S(2)}) %collective-permute-start.3) | collective-permute-done | bytes 262176 | tf_op jit(solution)/shard_map/ppermute | solution.py:29
  46.2 5.1 %collective-permute-start.15 = (bf16[64,2176]{1,0:T(8,128)(2,1)S(1)}, bf16[64,2176]{1,0:T(8,128)(2,1)S(1)}, u32[]{:S(2)}, u32[]{:S(2)}) collective-permute-start(bf16[64,2176]{1,0:T(8,128)(2,1)S(1)} %pad_maximum_fusion.8), channel_id=1, source_target_pairs={{0,4},{1,5},{2,6},{3,7},{4,0},{5,1},{6,2},{7,3},{8,12},{9,13},{10,... | collective-permute-start | bytes 835592 | tf_op jit(solution)/shard_map/ppermute | solution.py:29
  51.3 2.6 %collective-permute-start.5 = (bf16[64,2176]{1,0:T(8,128)(2,1)S(1)}, bf16[64,2176]{1,0:T(8,128)(2,1)S(1)}, u32[]{:S(2)}, u32[]{:S(2)}) collective-permute-start(bf16[64,2176]{1,0:T(8,128)(2,1)S(1)} %pad_maximum_fusion.8), channel_id=1, source_target_pairs={{0,2},{1,3},{2,4},{3,5},{4,6},{5,7},{6,0},{7,1},{8,10},{9,11},{10,... | collective-permute-start | bytes 835592 | tf_op jit(solution)/shard_map/ppermute | solution.py:29
  55.1 15.6 %collective-permute-done.15 = bf16[64,2176]{1,0:T(8,128)(2,1)S(1)} collective-permute-done((bf16[64,2176]{1,0:T(8,128)(2,1)S(1)}, bf16[64,2176]{1,0:T(8,128)(2,1)S(1)}, u32[]{:S(2)}, u32[]{:S(2)}) %collective-permute-start.15) | collective-permute-done | bytes 278560 | tf_op jit(solution)/shard_map/ppermute | solution.py:29
  82.2 3.0 %collective-permute-start.8 = (bf16[72,2048]{1,0:T(8,128)(2,1)S(1)}, bf16[72,2048]{1,0:T(8,128)(2,1)S(1)}, u32[]{:S(2)}, u32[]{:S(2)}) collective-permute-start(bf16[72,2048]{1,0:T(8,128)(2,1)S(1)} %get-tuple-element.38), channel_id=1, source_target_pairs={{0,24},{8,16},{16,8},{24,0},{1,25},{9,17},{17,9},{25,1},{2,26},{10... | collective-permute-start | bytes 884744 | tf_op jit(solution)/shard_map/ppermute | solution.py:39
  85.1 4.9 %collective-permute-done.18 = bf16[72,2048]{1,0:T(8,128)(2,1)S(1)} collective-permute-done((bf16[72,2048]{1,0:T(8,128)(2,1)S(1)}, bf16[72,2048]{1,0:T(8,128)(2,1)S(1)}, u32[]{:S(2)}, u32[]{:S(2)}) %collective-permute-start.18) | collective-permute-done | bytes 294944 | tf_op jit(solution)/shard_map/ppermute | solution.py:39
  91.1 3.7 %collective-permute-done.6 = bf16[72,2048]{1,0:T(8,128)(2,1)S(1)} collective-permute-done((bf16[72,2048]{1,0:T(8,128)(2,1)S(1)}, bf16[72,2048]{1,0:T(8,128)(2,1)S(1)}, u32[]{:S(2)}, u32[]{:S(2)}) %collective-permute-start.6) | collective-permute-done | bytes 294944 | tf_op jit(solution)/shard_map/ppermute | solution.py:39
  94.8 4.9 %collective-permute-done.7 = bf16[72,2048]{1,0:T(8,128)(2,1)S(1)} collective-permute-done((bf16[72,2048]{1,0:T(8,128)(2,1)S(1)}, bf16[72,2048]{1,0:T(8,128)(2,1)S(1)}, u32[]{:S(2)}, u32[]{:S(2)}) %collective-permute-start.7) | collective-permute-done | bytes 294944 | tf_op jit(solution)/shard_map/ppermute | solution.py:39
  106.3 4.0 %fusion.4 = f32[576,896]{1,0:T(8,128)} fusion(bf16[576,2048]{1,0:T(8,128)(2,1)S(1)} %constant_dynamic-update-slice_fusion.7, bf16[1,2048,896]{2,1,0:T(8,128)(2,1)S(1)} %copy-done.11), kind=kOutput, calls=%fused_computation.4 | convolution fusion | flops 2113929216 | bytes 8093696 | tf_op jit(solution)/shard_map/dot_general | solution.py:222
  110.2 11.0 %fusion.15 = bf16[576,2048]{1,0:T(8,128)(2,1)} fusion(bf16[1,896,2048]{2,1,0:T(8,128)(2,1)} %param.25, f32[576,896]{1,0:T(8,128)} %fusion.4, bf16[576,2048]{1,0:T(8,128)(2,1)} %copy-done.4, bf16[1,2048,896]{2,1,0:T(8,128)(2,1)} %param.23), kind=kOutput, calls=%fused_computation.13 | convolution fusion | flops 4232134656 | bytes 14123008 | tf_op jit(solution)/shard_map/dot_general | solution.py:224
  121.2 2.6 %slice.280 = bf16[288,2048]{1,0:T(8,128)(2,1)} slice(bf16[576,2048]{1,0:T(8,128)(2,1)} %fusion.15), slice={[288:576], [0:2048]} | slice | bytes 2359296 | tf_op jit(solution)/shard_map/slice | solution.py:227
  127.1 6.0 %fusion.6 = f32[576,896]{1,0:T(8,128)} fusion(bf16[576,2048]{1,0:T(8,128)(2,1)S(1)} %constant_dynamic-update-slice_fusion, bf16[1,2048,896]{2,1,0:T(8,128)(2,1)} %param.24), kind=kOutput, calls=%fused_computation.6 | convolution fusion | flops 2113929216 | bytes 8093696 | tf_op jit(solution)/shard_map/dot_general | solution.py:222
  133.1 11.2 %fusion.12 = bf16[576,2048]{1,0:T(8,128)(2,1)} fusion(bf16[1,896,2048]{2,1,0:T(8,128)(2,1)} %param.25, f32[576,896]{1,0:T(8,128)} %fusion.6, bf16[576,2048]{1,0:T(8,128)(2,1)} %copy-done.7, bf16[1,2048,896]{2,1,0:T(8,128)(2,1)} %param.23), kind=kOutput, calls=%fused_computation.12 | convolution fusion | flops 4232134656 | bytes 14123008 | tf_op jit(solution)/shard_map/dot_general | solution.py:224
  153.5 3.5 %collective-permute-done.22 = bf16[72,2048]{1,0:T(8,128)(2,1)S(1)} collective-permute-done((bf16[72,2048]{1,0:T(8,128)(2,1)S(1)}, bf16[72,2048]{1,0:T(8,128)(2,1)S(1)}, u32[]{:S(2)}, u32[]{:S(2)}) %collective-permute-start.22) | collective-permute-done | bytes 294944 | tf_op jit(solution)/shard_map/ppermute | solution.py:39
  158.7 5.2 %collective-permute-done.23 = bf16[72,2048]{1,0:T(8,128)(2,1)S(1)} collective-permute-done((bf16[72,2048]{1,0:T(8,128)(2,1)S(1)}, bf16[72,2048]{1,0:T(8,128)(2,1)S(1)}, u32[]{:S(2)}, u32[]{:S(2)}) %collective-permute-start.23) | collective-permute-done | bytes 294944 | tf_op jit(solution)/shard_map/ppermute | solution.py:39
  165.0 9.2 %collective-permute-start.25 = (bf16[64,2048]{1,0:T(8,128)(2,1)S(1)}, bf16[64,2048]{1,0:T(8,128)(2,1)S(1)}, u32[]{:S(2)}, u32[]{:S(2)}) collective-permute-start(bf16[64,2048]{1,0:T(8,128)(2,1)S(1)} %get-tuple-element.44), channel_id=1, source_target_pairs={{0,4},{1,5},{2,6},{3,7},{4,0},{5,1},{6,2},{7,3},{8,12},{9,13},{10,... | collective-permute-start | bytes 786440 | tf_op jit(solution)/shard_map/ppermute | solution.py:29
  176.9 3.3 %collective-permute-start.14 = (bf16[64,2048]{1,0:T(8,128)(2,1)S(1)}, bf16[64,2048]{1,0:T(8,128)(2,1)S(1)}, u32[]{:S(2)}, u32[]{:S(2)}) collective-permute-start(bf16[64,2048]{1,0:T(8,128)(2,1)S(1)} %slice.352), channel_id=1, source_target_pairs={{0,6},{1,7},{2,0},{3,1},{4,2},{5,3},{6,4},{7,5},{8,14},{9,15},{10,... | collective-permute-start | bytes 786440 | tf_op jit(solution)/shard_map/ppermute | solution.py:29
  180.2 10.8 %collective-permute-done.25 = bf16[64,2048]{1,0:T(8,128)(2,1)S(1)} collective-permute-done((bf16[64,2048]{1,0:T(8,128)(2,1)S(1)}, bf16[64,2048]{1,0:T(8,128)(2,1)S(1)}, u32[]{:S(2)}, u32[]{:S(2)}) %collective-permute-start.25) | collective-permute-done | bytes 262176 | tf_op jit(solution)/shard_map/ppermute | solution.py:29
  191.1 5.3 %collective-permute-done.14 = bf16[64,2048]{1,0:T(8,128)(2,1)S(1)} collective-permute-done((bf16[64,2048]{1,0:T(8,128)(2,1)S(1)}, bf16[64,2048]{1,0:T(8,128)(2,1)S(1)}, u32[]{:S(2)}, u32[]{:S(2)}) %collective-permute-start.14) | collective-permute-done | bytes 262176 | tf_op jit(solution)/shard_map/ppermute | solution.py:29
  (133 shorter events, 55.4 us)
Async XLA Ops:
  22.8 11.2 %collective-permute-start.2 = (bf16[64,2048]{1,0:T(8,128)(2,1)S(1)}, bf16[64,2048]{1,0:T(8,128)(2,1)S(1)}, u32[]{:S(2)}, u32[]{:S(2)}) collective-permute-start(bf16[64,2048]{1,0:T(8,128)(2,1)S(1)} %get-tuple-element.41), channel_id=1, source_target_pairs={{0,2},{1,3},{2,4},{3,5},{4,6},{5,7},{6,0},{7,1},{8,10},{9,11},{10,... | collective-permute-start | bytes 786440 | tf_op jit(solution)/shard_map/ppermute | solution.py:29
  24.4 20.0 %collective-permute-start.3 = (bf16[64,2048]{1,0:T(8,128)(2,1)S(1)}, bf16[64,2048]{1,0:T(8,128)(2,1)S(1)}, u32[]{:S(2)}, u32[]{:S(2)}) collective-permute-start(bf16[64,2048]{1,0:T(8,128)(2,1)S(1)} %get-tuple-element.42), channel_id=1, source_target_pairs={{0,4},{1,5},{2,6},{3,7},{4,0},{5,1},{6,2},{7,3},{8,12},{9,13},{10,... | collective-permute-start | bytes 786440 | tf_op jit(solution)/shard_map/ppermute | solution.py:29
  27.0 17.4 %collective-permute-start.4 = (bf16[64,2048]{1,0:T(8,128)(2,1)S(1)}, bf16[64,2048]{1,0:T(8,128)(2,1)S(1)}, u32[]{:S(2)}, u32[]{:S(2)}) collective-permute-start(bf16[64,2048]{1,0:T(8,128)(2,1)S(1)} %get-tuple-element.43), channel_id=1, source_target_pairs={{0,6},{1,7},{2,0},{3,1},{4,2},{5,3},{6,4},{7,5},{8,14},{9,15},{10,... | collective-permute-start | bytes 786440 | tf_op jit(solution)/shard_map/ppermute | solution.py:29
  46.2 24.6 %collective-permute-start.15 = (bf16[64,2176]{1,0:T(8,128)(2,1)S(1)}, bf16[64,2176]{1,0:T(8,128)(2,1)S(1)}, u32[]{:S(2)}, u32[]{:S(2)}) collective-permute-start(bf16[64,2176]{1,0:T(8,128)(2,1)S(1)} %pad_maximum_fusion.8), channel_id=1, source_target_pairs={{0,4},{1,5},{2,6},{3,7},{4,0},{5,1},{6,2},{7,3},{8,12},{9,13},{10,... | collective-permute-start | bytes 835592 | tf_op jit(solution)/shard_map/ppermute | solution.py:29
  51.3 19.5 %collective-permute-start.5 = (bf16[64,2176]{1,0:T(8,128)(2,1)S(1)}, bf16[64,2176]{1,0:T(8,128)(2,1)S(1)}, u32[]{:S(2)}, u32[]{:S(2)}) collective-permute-start(bf16[64,2176]{1,0:T(8,128)(2,1)S(1)} %pad_maximum_fusion.8), channel_id=1, source_target_pairs={{0,2},{1,3},{2,4},{3,5},{4,6},{5,7},{6,0},{7,1},{8,10},{9,11},{10,... | collective-permute-start | bytes 835592 | tf_op jit(solution)/shard_map/ppermute | solution.py:29
  53.9 16.9 %collective-permute-start.16 = (bf16[64,2176]{1,0:T(8,128)(2,1)S(1)}, bf16[64,2176]{1,0:T(8,128)(2,1)S(1)}, u32[]{:S(2)}, u32[]{:S(2)}) collective-permute-start(bf16[64,2176]{1,0:T(8,128)(2,1)S(1)} %pad_maximum_fusion.8), channel_id=1, source_target_pairs={{0,6},{1,7},{2,0},{3,1},{4,2},{5,3},{6,4},{7,5},{8,14},{9,15},{10,... | collective-permute-start | bytes 835592 | tf_op jit(solution)/shard_map/ppermute | solution.py:29
  71.9 10.3 %collective-permute-start.17 = (bf16[72,2048]{1,0:T(8,128)(2,1)S(1)}, bf16[72,2048]{1,0:T(8,128)(2,1)S(1)}, u32[]{:S(2)}, u32[]{:S(2)}) collective-permute-start(bf16[72,2048]{1,0:T(8,128)(2,1)S(1)} %get-tuple-element.31), channel_id=1, source_target_pairs={{0,8},{8,0},{16,24},{24,16},{1,9},{9,1},{17,25},{25,17},{2,10},{10... | collective-permute-start | bytes 884744 | tf_op jit(solution)/shard_map/ppermute | solution.py:39
  74.3 15.8 %collective-permute-start.18 = (bf16[72,2048]{1,0:T(8,128)(2,1)S(1)}, bf16[72,2048]{1,0:T(8,128)(2,1)S(1)}, u32[]{:S(2)}, u32[]{:S(2)}) collective-permute-start(bf16[72,2048]{1,0:T(8,128)(2,1)S(1)} %get-tuple-element.30), channel_id=1, source_target_pairs={{0,16},{8,24},{16,0},{24,8},{1,17},{9,25},{17,1},{25,9},{2,18},{10... | collective-permute-start | bytes 884744 | tf_op jit(solution)/shard_map/ppermute | solution.py:39
  75.8 15.1 %collective-permute-start.19 = (bf16[72,2048]{1,0:T(8,128)(2,1)S(1)}, bf16[72,2048]{1,0:T(8,128)(2,1)S(1)}, u32[]{:S(2)}, u32[]{:S(2)}) collective-permute-start(bf16[72,2048]{1,0:T(8,128)(2,1)S(1)} %get-tuple-element.29), channel_id=1, source_target_pairs={{0,24},{8,16},{16,8},{24,0},{1,25},{9,17},{17,9},{25,1},{2,26},{10... | collective-permute-start | bytes 884744 | tf_op jit(solution)/shard_map/ppermute | solution.py:39
  77.7 17.2 %collective-permute-start.6 = (bf16[72,2048]{1,0:T(8,128)(2,1)S(1)}, bf16[72,2048]{1,0:T(8,128)(2,1)S(1)}, u32[]{:S(2)}, u32[]{:S(2)}) collective-permute-start(bf16[72,2048]{1,0:T(8,128)(2,1)S(1)} %get-tuple-element.40), channel_id=1, source_target_pairs={{0,8},{8,0},{16,24},{24,16},{1,9},{9,1},{17,25},{25,17},{2,10},{10... | collective-permute-start | bytes 884744 | tf_op jit(solution)/shard_map/ppermute | solution.py:39
  78.8 20.9 %collective-permute-start.7 = (bf16[72,2048]{1,0:T(8,128)(2,1)S(1)}, bf16[72,2048]{1,0:T(8,128)(2,1)S(1)}, u32[]{:S(2)}, u32[]{:S(2)}) collective-permute-start(bf16[72,2048]{1,0:T(8,128)(2,1)S(1)} %get-tuple-element.39), channel_id=1, source_target_pairs={{0,16},{8,24},{16,0},{24,8},{1,17},{9,25},{17,1},{25,9},{2,18},{10... | collective-permute-start | bytes 884744 | tf_op jit(solution)/shard_map/ppermute | solution.py:39
  82.2 19.2 %collective-permute-start.8 = (bf16[72,2048]{1,0:T(8,128)(2,1)S(1)}, bf16[72,2048]{1,0:T(8,128)(2,1)S(1)}, u32[]{:S(2)}, u32[]{:S(2)}) collective-permute-start(bf16[72,2048]{1,0:T(8,128)(2,1)S(1)} %get-tuple-element.38), channel_id=1, source_target_pairs={{0,24},{8,16},{16,8},{24,0},{1,25},{9,17},{17,9},{25,1},{2,26},{10... | collective-permute-start | bytes 884744 | tf_op jit(solution)/shard_map/ppermute | solution.py:39
  91.0 11.6 %collective-permute-start.20 = (bf16[288,2048]{1,0:T(8,128)(2,1)S(1)}, bf16[288,2048]{1,0:T(8,128)(2,1)S(1)}, u32[]{:S(2)}, u32[]{:S(2)}) collective-permute-start(bf16[288,2048]{1,0:T(8,128)(2,1)S(1)} %pad_maximum_fusion.2), channel_id=1, source_target_pairs={{0,1},{1,0},{2,3},{3,2},{4,5},{5,4},{6,7},{7,6},{8,9},{9,8},{10,11... | collective-permute-start | bytes 3538952 | tf_op jit(solution)/shard_map/ppermute | solution.py:35
  102.5 21.9 %collective-permute-start.9 = (bf16[288,2048]{1,0:T(8,128)(2,1)}, bf16[288,2048]{1,0:T(8,128)(2,1)}, u32[]{:S(2)}, u32[]{:S(2)}) collective-permute-start(bf16[288,2048]{1,0:T(8,128)(2,1)} %pad_maximum_fusion), channel_id=1, source_target_pairs={{0,1},{1,0},{2,3},{3,2},{4,5},{5,4},{6,7},{7,6},{8,9},{9,8},{10,11... | collective-permute-start | bytes 3538952 | tf_op jit(solution)/shard_map/ppermute | solution.py:35
  123.8 22.6 %collective-permute-start.21 = (bf16[288,2048]{1,0:T(8,128)(2,1)}, bf16[288,2048]{1,0:T(8,128)(2,1)S(1)}, u32[]{:S(2)}, u32[]{:S(2)}) collective-permute-start(bf16[288,2048]{1,0:T(8,128)(2,1)} %slice.280), channel_id=1, source_target_pairs={{0,1},{1,0},{2,3},{3,2},{4,5},{5,4},{6,7},{7,6},{8,9},{9,8},{10,11... | collective-permute-start | bytes 3538952 | tf_op jit(solution)/shard_map/ppermute | solution.py:35
  147.0 9.9 %collective-permute-start.22 = (bf16[72,2048]{1,0:T(8,128)(2,1)S(1)}, bf16[72,2048]{1,0:T(8,128)(2,1)S(1)}, u32[]{:S(2)}, u32[]{:S(2)}) collective-permute-start(bf16[72,2048]{1,0:T(8,128)(2,1)S(1)} %get-tuple-element.26), channel_id=1, source_target_pairs={{0,8},{8,0},{16,24},{24,16},{1,9},{9,1},{17,25},{25,17},{2,10},{10... | collective-permute-start | bytes 884744 | tf_op jit(solution)/shard_map/ppermute | solution.py:39
  147.7 16.2 %collective-permute-start.23 = (bf16[72,2048]{1,0:T(8,128)(2,1)S(1)}, bf16[72,2048]{1,0:T(8,128)(2,1)S(1)}, u32[]{:S(2)}, u32[]{:S(2)}) collective-permute-start(bf16[72,2048]{1,0:T(8,128)(2,1)S(1)} %get-tuple-element.25), channel_id=1, source_target_pairs={{0,16},{8,24},{16,0},{24,8},{1,17},{9,25},{17,1},{25,9},{2,18},{10... | collective-permute-start | bytes 884744 | tf_op jit(solution)/shard_map/ppermute | solution.py:39
  149.4 14.5 %collective-permute-start.24 = (bf16[72,2048]{1,0:T(8,128)(2,1)S(1)}, bf16[72,2048]{1,0:T(8,128)(2,1)S(1)}, u32[]{:S(2)}, u32[]{:S(2)}) collective-permute-start(bf16[72,2048]{1,0:T(8,128)(2,1)S(1)} %get-tuple-element.24), channel_id=1, source_target_pairs={{0,24},{8,16},{16,8},{24,0},{1,25},{9,17},{17,9},{25,1},{2,26},{10... | collective-permute-start | bytes 884744 | tf_op jit(solution)/shard_map/ppermute | solution.py:39
  151.2 23.0 %collective-permute-start.11 = (bf16[72,2048]{1,0:T(8,128)(2,1)S(1)}, bf16[72,2048]{1,0:T(8,128)(2,1)S(1)}, u32[]{:S(2)}, u32[]{:S(2)}) collective-permute-start(bf16[72,2048]{1,0:T(8,128)(2,1)S(1)} %get-tuple-element.35), channel_id=1, source_target_pairs={{0,8},{8,0},{16,24},{24,16},{1,9},{9,1},{17,25},{25,17},{2,10},{10... | collective-permute-start | bytes 884744 | tf_op jit(solution)/shard_map/ppermute | solution.py:39
  151.8 23.2 %collective-permute-start.12 = (bf16[72,2048]{1,0:T(8,128)(2,1)S(1)}, bf16[72,2048]{1,0:T(8,128)(2,1)S(1)}, u32[]{:S(2)}, u32[]{:S(2)}) collective-permute-start(bf16[72,2048]{1,0:T(8,128)(2,1)S(1)} %get-tuple-element.34), channel_id=1, source_target_pairs={{0,16},{8,24},{16,0},{24,8},{1,17},{9,25},{17,1},{25,9},{2,18},{10... | collective-permute-start | bytes 884744 | tf_op jit(solution)/shard_map/ppermute | solution.py:39
  157.0 18.8 %collective-permute-start.13 = (bf16[72,2048]{1,0:T(8,128)(2,1)S(1)}, bf16[72,2048]{1,0:T(8,128)(2,1)S(1)}, u32[]{:S(2)}, u32[]{:S(2)}) collective-permute-start(bf16[72,2048]{1,0:T(8,128)(2,1)S(1)} %get-tuple-element.33), channel_id=1, source_target_pairs={{0,24},{8,16},{16,8},{24,0},{1,25},{9,17},{17,9},{25,1},{2,26},{10... | collective-permute-start | bytes 884744 | tf_op jit(solution)/shard_map/ppermute | solution.py:39
  165.0 26.1 %collective-permute-start.25 = (bf16[64,2048]{1,0:T(8,128)(2,1)S(1)}, bf16[64,2048]{1,0:T(8,128)(2,1)S(1)}, u32[]{:S(2)}, u32[]{:S(2)}) collective-permute-start(bf16[64,2048]{1,0:T(8,128)(2,1)S(1)} %get-tuple-element.44), channel_id=1, source_target_pairs={{0,4},{1,5},{2,6},{3,7},{4,0},{5,1},{6,2},{7,3},{8,12},{9,13},{10,... | collective-permute-start | bytes 786440 | tf_op jit(solution)/shard_map/ppermute | solution.py:29
  174.2 16.9 %collective-permute-start.26 = (bf16[64,2048]{1,0:T(8,128)(2,1)S(1)}, bf16[64,2048]{1,0:T(8,128)(2,1)S(1)}, u32[]{:S(2)}, u32[]{:S(2)}) collective-permute-start(bf16[64,2048]{1,0:T(8,128)(2,1)S(1)} %get-tuple-element.45), channel_id=1, source_target_pairs={{0,2},{1,3},{2,4},{3,5},{4,6},{5,7},{6,0},{7,1},{8,10},{9,11},{10,... | collective-permute-start | bytes 786440 | tf_op jit(solution)/shard_map/ppermute | solution.py:29
  176.9 19.5 %collective-permute-start.14 = (bf16[64,2048]{1,0:T(8,128)(2,1)S(1)}, bf16[64,2048]{1,0:T(8,128)(2,1)S(1)}, u32[]{:S(2)}, u32[]{:S(2)}) collective-permute-start(bf16[64,2048]{1,0:T(8,128)(2,1)S(1)} %slice.352), channel_id=1, source_target_pairs={{0,6},{1,7},{2,0},{3,1},{4,2},{5,3},{6,4},{7,5},{8,14},{9,15},{10,... | collective-permute-start | bytes 786440 | tf_op jit(solution)/shard_map/ppermute | solution.py:29
  (15 other events, 111.0 us)
